TPU v7x, 32 devices: a whole 2x2x4 slice. The times are simulated.
32 devices in a mesh: sp: 8 (over z, x), dp: 4 (over y, core).
Axes of the slice: x: 2, y: 2, z: 4, core: 2. Of those that a mesh axis runs over, the one named last changes fastest.
Arguments:
- query_rows: bfloat16 [4, 1024, 2048], P('dp', 'sp'), may hold values from -6 to 6
- key_rows: bfloat16 [4, 1024, 2048], P('dp', 'sp'), may hold values from -6 to 6
- value_rows: bfloat16 [4, 1024, 2048], P('dp', 'sp'), may hold values from -6 to 6
- decay_low: bfloat16 [4, 1024, 128], P('dp', 'sp'), may hold values from -5 to 5
- rate_low: bfloat16 [4, 1024, 128], P('dp', 'sp'), may hold values from -4 to 4
- decay_up: bfloat16 [128, 2048], replicated, may hold values from -0.5 to 0.5
- rate_up: bfloat16 [128, 2048], replicated, may hold values from -0.5 to 0.5
- decay_base: float32 [2048], replicated, may hold values from -12 to -2
- norm_gain: float32 [2048], replicated, may hold values from 0.1 to 1.9
- out_weight: bfloat16 [2048, 2048], P(None, 'dp'), may hold values from -0.125 to 0.125
Outputs:
- layer_out: bfloat16 [4, 1024, 2048], P('dp', 'sp')
All inputs are finite; a program needn't handle non-finite values.
Results may differ from a plain program's by a relative error of at most 0.005.
Values may be sent and summed in bfloat16 or wider, within the bound.
A program may use at most 128 MiB of HBM per device.

v0:
```python
import math

import jax
import jax.numpy as jnp
from jax import lax
from jax.sharding import PartitionSpec as P

HEAD = 64


HIGHEST = lax.Precision.HIGHEST
THREE_PASS = lax.Precision.HIGH


def product(form, left, right):
    return jnp.einsum(form, left, right, precision=HIGHEST)


def product_three(form, left, right):
    return jnp.einsum(form, left, right, precision=THREE_PASS)


def to_blocks(rows, heads, block_len):
    positions = rows.shape[0]
    return rows.reshape(positions // block_len, block_len, heads, -1).transpose(2, 0, 3, 1)


def compose(earlier, later):
    return (
        product("hbij,hbjk->hbik", later[0], earlier[0]),
        product("hbij,hbjk->hbik", later[0], earlier[1]) + later[1],
    )


def pre_gates(low_decay, low_rate, decay_up, rate_up, decay_base):
    squashed = jnp.tanh(low_decay.astype(jnp.float32)).astype(jnp.bfloat16)
    decay_pre = (
        decay_base + jnp.dot(squashed, decay_up, preferred_element_type=jnp.float32)
    ).astype(jnp.bfloat16)
    rate_pre = jnp.dot(low_rate, rate_up, preferred_element_type=jnp.float32).astype(jnp.bfloat16)
    return (decay_pre, rate_pre)


def run_mixer(reads, keyed, valued, decay_in, rate_in, gain_here):
    positions = reads.shape[0]
    heads = reads.shape[1] // HEAD
    block_len = math.gcd(positions, 128)
    middle = block_len // 2
    query_blocks = to_blocks(reads.astype(jnp.float32), heads, block_len)
    key_blocks = to_blocks(keyed.astype(jnp.float32), heads, block_len)
    value_blocks = to_blocks(valued.astype(jnp.float32), heads, block_len)
    log_decay = -jnp.exp(-jax.nn.softplus(-decay_in.astype(jnp.float32)) - 0.5)
    decay_blocks = to_blocks(log_decay, heads, block_len)
    rate_blocks = to_blocks(jax.nn.sigmoid(rate_in.astype(jnp.float32)), heads, block_len)
    unit_keys = key_blocks * lax.rsqrt(
        1.0 + jnp.sum(key_blocks * key_blocks, axis=2, keepdims=True)
    )
    erase = unit_keys * rate_blocks
    row_index = lax.broadcasted_iota(jnp.int32, (block_len, block_len), 0)
    col_index = lax.broadcasted_iota(jnp.int32, (block_len, block_len), 1)
    upper = (row_index <= col_index).astype(jnp.float32)
    running = product("hbnc,cd->hbnd", decay_blocks, upper)
    before = running - decay_blocks
    centre = running[..., middle : middle + 1]
    final = running[..., block_len - 1 :]
    read_mid = query_blocks * jnp.exp(running - centre)
    erase_from = unit_keys * jnp.exp(before - centre)
    key_to = key_blocks * jnp.exp(centre - running)
    erase_to = erase * jnp.exp(centre - running)
    read_start = query_blocks * jnp.exp(running)
    erase_start = unit_keys * jnp.exp(before)
    key_end = key_blocks * jnp.exp(final - running)
    erase_end = erase * jnp.exp(final - running)
    strict = row_index > col_index
    within = row_index >= col_index
    key_pairs = jnp.where(strict, product_three("hbnt,hbns->hbts", erase_from, key_to), 0.0)
    erase_pairs = jnp.where(strict, product("hbnt,hbns->hbts", erase_from, erase_to), 0.0)
    read_keys = jnp.where(within, product_three("hbnt,hbns->hbts", read_mid, key_to), 0.0)
    read_erase = jnp.where(within, product_three("hbnt,hbns->hbts", read_mid, erase_to), 0.0)
    lower_matrix = jnp.eye(block_len, dtype=jnp.float32) + erase_pairs
    carried = product_three("hbts,hbms->hbtm", key_pairs, value_blocks)
    right_sides = jnp.concatenate([jnp.swapaxes(erase_start, 2, 3), carried], axis=-1)
    solved = jax.scipy.linalg.solve_triangular(
        lower_matrix, right_sides, lower=True, unit_diagonal=True
    )
    start_weights = solved[..., :HEAD]
    local_erase = solved[..., HEAD:]
    transfer = jnp.eye(HEAD, dtype=jnp.float32) * jnp.exp(final) - product_three(
        "hbnt,hbtk->hbnk", erase_end, start_weights
    )
    added = product_three("hbnt,hbmt->hbnm", key_end, value_blocks) - product_three(
        "hbnt,hbtm->hbnm", erase_end, local_erase
    )
    _, ends = lax.associative_scan(compose, (transfer, added), axis=1)
    starts = jnp.concatenate([jnp.zeros_like(ends[:, :1]), ends[:, :-1]], axis=1)
    read_state = jnp.swapaxes(read_start, 2, 3) - product_three(
        "hbts,hbsn->hbtn", read_erase, start_weights
    )
    readout = (
        product_three("hbtn,hbnm->hbtm", read_state, starts)
        + product_three("hbts,hbms->hbtm", read_keys, value_blocks)
        - product_three("hbts,hbsm->hbtm", read_erase, local_erase)
    )
    average = jnp.mean(readout, axis=-1, keepdims=True)
    centred = readout - average
    variance = jnp.mean(centred * centred, axis=-1, keepdims=True)
    normed = centred * lax.rsqrt(variance + 1.0)
    rows_out = normed.transpose(1, 2, 0, 3).reshape(positions, heads * HEAD)
    return (rows_out * gain_here).astype(jnp.bfloat16)


def per_device(
    query_rows,
    key_rows,
    value_rows,
    decay_low,
    rate_low,
    decay_up,
    rate_up,
    decay_base,
    norm_gain,
    out_weight,
):
    reads = query_rows[0]
    keyed = key_rows[0]
    valued = value_rows[0]
    got_reads, got_keys, got_values = (
        lax.all_to_all(reads, "sp", split_axis=1, concat_axis=0, tiled=True),
        lax.all_to_all(keyed, "sp", split_axis=1, concat_axis=0, tiled=True),
        lax.all_to_all(valued, "sp", split_axis=1, concat_axis=0, tiled=True),
    )
    decay_pre, rate_pre = pre_gates(decay_low[0], rate_low[0], decay_up, rate_up, decay_base)
    got_decay, got_rate = (
        lax.all_to_all(decay_pre, "sp", split_axis=1, concat_axis=0, tiled=True),
        lax.all_to_all(rate_pre, "sp", split_axis=1, concat_axis=0, tiled=True),
    )
    width_here = got_reads.shape[1]
    gain_here = lax.dynamic_slice_in_dim(norm_gain, lax.axis_index("sp") * width_here, width_here)
    mix = run_mixer(got_reads, got_keys, got_values, got_decay, got_rate, gain_here)
    back = lax.all_to_all(mix, "sp", split_axis=0, concat_axis=1, tiled=True)
    layer_out = jnp.dot(
        back,
        lax.all_gather(out_weight, "dp", axis=1, tiled=True),
        preferred_element_type=jnp.float32,
    ).astype(jnp.bfloat16)
    return layer_out[None]


def solution(mesh):
    in_specs = (
        P("dp", "sp", None),
        P("dp", "sp", None),
        P("dp", "sp", None),
        P("dp", "sp", None),
        P("dp", "sp", None),
        P(),
        P(),
        P(),
        P(),
        P(None, "dp"),
    )
    out_specs = P("dp", "sp", None)
    return jax.shard_map(
        per_device, mesh=mesh, in_specs=in_specs, out_specs=out_specs, check_vma=False
    )
```

profile of v0, /device:TPU:30, one launch (start us, length us, event | category | flops | bytes accessed | tf_op | source)
XLA Modules:
  0.0 499.1 jit_solution(11497053857221904413)
XLA Ops:
  6.5 2.1 copy.22
  8.6 6.0 %all-to-all-start.2 = ((bf16[128,8,256]{0,2,1:T(8,128)(2,1)}), bf16[128,8,256]{0,2,1:T(8,128)(2,1)S(1)}, u32[]{:S(2)}, u32[]{:S(2)}) async-start(bf16[128,8,256]{0,2,1:T(8,128)(2,1)} %bitcast.15), calls=%async_computation.2 | async-start | bytes 1048576 | tf_op jit(solution)/shard_map/all_to_all | solution.py:129
  14.6 0.7 all-gather.2.cloned.1.call-update
  15.4 0.3 fusion
  15.7 1.0 copy.35
  16.8 10.0 %all-to-all-done.2 = bf16[128,8,256]{0,2,1:T(8,128)(2,1)S(1)} async-done(((bf16[128,8,256]{0,2,1:T(8,128)(2,1)}), bf16[128,8,256]{0,2,1:T(8,128)(2,1)S(1)}, u32[]{:S(2)}, u32[]{:S(2)}) %all-to-all-start.2) | async-done | bytes 524320 | tf_op jit(solution)/shard_map/all_to_all | solution.py:129
  26.8 6.0 %all-to-all-start.1 = ((bf16[128,8,256]{0,2,1:T(8,128)(2,1)}), bf16[128,8,256]{0,2,1:T(8,128)(2,1)S(1)}, u32[]{:S(2)}, u32[]{:S(2)}) async-start(bf16[128,8,256]{0,2,1:T(8,128)(2,1)} %bitcast.5), calls=%async_computation.1 | async-start | bytes 1048576 | tf_op jit(solution)/shard_map/all_to_all | solution.py:134
  32.8 0.3 convolution_convert_fusion.1
  33.1 1.0 copy.36
  34.1 10.9 %all-to-all-done.1 = bf16[128,8,256]{0,2,1:T(8,128)(2,1)S(1)} async-done(((bf16[128,8,256]{0,2,1:T(8,128)(2,1)}), bf16[128,8,256]{0,2,1:T(8,128)(2,1)S(1)}, u32[]{:S(2)}, u32[]{:S(2)}) %all-to-all-start.1) | async-done | bytes 524320 | tf_op jit(solution)/shard_map/all_to_all | solution.py:134
  45.1 6.0 %all-to-all-start.3 = ((bf16[128,8,256]{0,2,1:T(8,128)(2,1)}), bf16[128,8,256]{0,2,1:T(8,128)(2,1)S(1)}, u32[]{:S(2)}, u32[]{:S(2)}) async-start(bf16[128,8,256]{0,2,1:T(8,128)(2,1)} %bitcast.20), calls=%async_computation.3 | async-start | bytes 1048576 | tf_op jit(solution)/shard_map/all_to_all | solution.py:135
  51.1 2.1 copy.27
  53.1 1.0 copy.13
  54.2 0.8 dynamic_slice.3
  54.9 0.1 iota_compare_fusion.3
  55.0 0.1 convert_element_type.91
  55.1 0.1 fusion.34
  55.2 1.1 convert_negate_fusion
  56.3 7.1 %all-to-all-done.3 = bf16[128,8,256]{0,2,1:T(8,128)(2,1)S(1)} async-done(((bf16[128,8,256]{0,2,1:T(8,128)(2,1)}), bf16[128,8,256]{0,2,1:T(8,128)(2,1)S(1)}, u32[]{:S(2)}, u32[]{:S(2)}) %all-to-all-start.3) | async-done | bytes 524320 | tf_op jit(solution)/shard_map/all_to_all | solution.py:135
  63.4 6.0 %all-to-all-start.4 = ((bf16[128,8,256]{0,2,1:T(8,128)(2,1)}), bf16[128,8,256]{0,2,1:T(8,128)(2,1)S(1)}, u32[]{:S(2)}, u32[]{:S(2)}) async-start(bf16[128,8,256]{0,2,1:T(8,128)(2,1)} %bitcast.162), calls=%async_computation.4 | async-start | bytes 1048576 | tf_op jit(solution)/shard_map/all_to_all | solution.py:130
  69.4 0.3 add_divide_fusion
  69.7 0.2 bitcast_multiply_fusion.2
  69.9 0.7 copy-done.7
  70.6 3.0 fusion.33
  73.6 1.4 exponential_reduce_fusion
  75.0 5.8 %add_bitcast_fusion = f32[4,8,1,128,128]{4,3,2,1,0:T(8,128)} fusion(f32[128,128]{1,0:T(8,128)S(1)} %fusion.93, f32[128,128]{1,0:T(8,128)S(1)} %get-tuple-element.15, pred[128,128]{1,0:T(8,128)(4,1)S(1)} %iota_compare_fusion.1, pred[128,128]{1,0:T(8,128)(4,1)S(1)} %get-tuple-element.14, f32[4,8,64,128]{3,2,1,0:T(8,128)S(1)} %bitcast_multiply_fusion.2, ...), kind=kOutput, calls=%fused_computation.15 | convolution fusion | flops 408682496 | bytes 6479872 | tf_op jit(solution)/shard_map/hbnt,hbns->hbts/dot_general | solution.py:16
  80.9 315.8 %custom-call.4 = f32[4,8,1,128,128]{3,4,2,1,0:T(8,128)} custom-call(f32[4,8,1,128,128]{4,3,2,1,0:T(8,128)} %add_bitcast_fusion), custom_call_target="InvertDiagBlocksLowerTriangular" | custom-call | tf_op jit(solution)/shard_map/jit(_solve_triangular)/vmap(vmap())/triangular_solve | solution.py:83
  396.7 5.3 %fusion.81 = f32[4,8,128,128]{3,2,1,0:T(8,128)} fusion(f32[4,8,64,128]{3,2,1,0:T(8,128)S(1)} %get-tuple-element.11, f32[8,128,4,64]{1,3,2,0:T(8,128)S(1)} %bitcast.147, f32[4,8,64]{2,1,0:T(8,128)S(1)} %get-tuple-element.7, f32[4,8,128]{2,1,0:T(8,128)S(1)} %add_rsqrt_fusion, f32[8,128,4,64]{1,3,2,0:T(8,128)} %bitcast.157), kind=kOutput, calls=%fused_computation.108 | convolution fusion | flops 205258752 | bytes 5267456 | tf_op jit(solution)/shard_map/hbnt,hbns->hbts/dot_general | solution.py:20
  402.0 6.0 %all-to-all-start = ((bf16[128,8,256]{0,2,1:T(8,128)(2,1)}), bf16[128,8,256]{0,2,1:T(8,128)(2,1)}, u32[]{:S(2)}, u32[]{:S(2)}) async-start(bf16[128,8,256]{0,2,1:T(8,128)(2,1)} %bitcast.161), calls=%async_computation | async-start | bytes 1048576 | tf_op jit(solution)/shard_map/all_to_all | solution.py:128
  408.0 3.3 fusion.9
  411.3 0.0 copy-done.9
  411.3 2.2 fusion.2
  413.5 1.1 convolution_subtract_fusion
  414.6 0.7 fusion.62
  415.3 0.3 convolution_bitcast_fusion
  415.5 0.7 fusion.35
  416.3 1.1 convolution_subtract_fusion.1
  417.4 0.7 convolution_add_fusion.1
  418.0 0.4 convolution_add_fusion.3
  418.4 0.3 fusion.24
  418.8 0.3 fusion.25
  419.0 0.7 pad_maximum_fusion.1
  419.8 5.1 %pad.22 = f32[4,4,64,64]{3,2,1,0:T(8,128)} pad(f32[4,2,64,64]{3,2,1,0:T(8,128)} %pad_maximum_fusion.1, f32[]{:T(128)} %constant.12.clone.1), padding=0_0_0x0_1_1x0_0_0x0_0_0 | pad | bytes 393220 | tf_op jit(solution)/shard_map/pad | solution.py:94
  424.9 0.7 pad_add_fusion
  425.6 5.1 %pad.23 = f32[4,4,64,64]{3,2,1,0:T(8,128)} pad(f32[4,2,64,64]{3,2,1,0:T(8,128)} %pad_add_fusion, f32[]{:T(128)} %constant.12.clone.1), padding=0_0_0x1_0_1x0_0_0x0_0_0 | pad | bytes 393220 | tf_op jit(solution)/shard_map/pad | solution.py:94
  430.7 2.1 add.118
  432.8 9.2 %pad.59 = f32[4,8,64,64]{3,2,1,0:T(8,128)} pad(f32[4,4,64,64]{3,2,1,0:T(8,128)} %add.118, f32[]{:T(128)} %constant.12.clone.1), padding=0_0_0x1_0_1x0_0_0x0_0_0 | pad | bytes 786436
  442.0 1.9 convolution_add_fusion.2
  443.9 0.8 pad_maximum_fusion
  444.7 9.2 %pad.33 = f32[4,7,64,64]{3,2,1,0:T(8,128)} pad(f32[4,4,64,64]{3,2,1,0:T(8,128)} %pad_maximum_fusion, f32[]{:T(128)} %constant.12.clone.1), padding=0_0_0x0_0_1x0_0_0x0_0_0 | pad | bytes 720900 | tf_op jit(solution)/shard_map/slice | solution.py:95
  453.9 1.2 convert_element_type.90
  455.1 1.6 slice_add_fusion
  456.7 2.9 fusion.78
  459.6 2.2 fusion.15
  461.8 0.9 fusion.42
  462.7 2.6 fusion.80
  465.4 1.6 fusion.21
  467.0 2.2 fusion.110
  469.2 0.2 multiply_reduce_fusion
  469.4 0.2 fusion.31
  469.6 0.1 copy.31
  469.7 0.2 fusion.30
  469.8 17.0 %all_to_all.84 = bf16[8,128,256]{1,2,0:T(8,128)(2,1)S(1)} all-to-all(bf16[8,128,256]{1,2,0:T(8,128)(2,1)S(1)} %fusion.30), channel_id=1, replica_groups=mesh['sp'=8,'dp'=4] {'sp'}, dimensions={0} | all-to-all | bytes 1048576 | tf_op jit(solution)/shard_map/all_to_all | solution.py:140
  486.8 5.5 %fusion.1 = bf16[1,128,2048]{2,1,0:T(8,128)(2,1)} fusion(bf16[128,2048]{0,1:T(8,128)(2,1)S(1)} %bitcast.156, bf16[2048,2048]{1,0:T(8,128)(2,1)} %all-gather.2.cloned.1.call-done), kind=kOutput, calls=%fused_computation.5 | convolution fusion | flops 1074003968 | bytes 9437184 | tf_op jit(solution)/shard_map/dot_general | solution.py:141
  (46 shorter events, 0.2 us)
Async XLA Ops:
  6.5 8.8 %copy-start = (bf16[128,2048]{1,0:T(8,128)(2,1)S(1)}, bf16[128,2048]{1,0:T(8,128)(2,1)}, u32[]{:S(2)}) copy-start(bf16[128,2048]{1,0:T(8,128)(2,1)} %param.15) | copy-start | bytes 1572868
  6.5 8.8 %copy-start.13 = (bf16[1,128,128]{2,1,0:T(8,128)(2,1)S(1)}, bf16[1,128,128]{2,1,0:T(8,128)(2,1)}, u32[]{:S(2)}) copy-start(bf16[1,128,128]{2,1,0:T(8,128)(2,1)} %param.13) | copy-start | bytes 98308
  6.5 8.8 %copy-start.15 = (f32[2048]{0:T(1024)S(1)}, f32[2048]{0:T(1024)}, u32[]{:S(2)}) copy-start(f32[2048]{0:T(1024)} %param.17) | copy-start | bytes 24580
  8.6 18.1 %all-to-all-start.2 = ((bf16[128,8,256]{0,2,1:T(8,128)(2,1)}), bf16[128,8,256]{0,2,1:T(8,128)(2,1)S(1)}, u32[]{:S(2)}, u32[]{:S(2)}) async-start(bf16[128,8,256]{0,2,1:T(8,128)(2,1)} %bitcast.15), calls=%async_computation.2 | async-start | bytes 1048576 | tf_op jit(solution)/shard_map/all_to_all | solution.py:129
  14.6 472.2 %all-gather.2.cloned.1.call-start = ((), (), s32[]{:S(2)}) async-start(), calls=%async_computation.6 | async-start | bytes 10485760 | tf_op jit(solution)/shard_map/all_gather | solution.py:143
  15.4 17.4 %copy-start.11 = (bf16[128,2048]{1,0:T(8,128)(2,1)S(1)}, bf16[128,2048]{1,0:T(8,128)(2,1)}, u32[]{:S(2)}) copy-start(bf16[128,2048]{1,0:T(8,128)(2,1)} %param.16) | copy-start | bytes 1572868
  15.4 17.4 %copy-start.14 = (bf16[1,128,128]{2,1,0:T(8,128)(2,1)S(1)}, bf16[1,128,128]{2,1,0:T(8,128)(2,1)}, u32[]{:S(2)}) copy-start(bf16[1,128,128]{2,1,0:T(8,128)(2,1)} %param.14) | copy-start | bytes 98308
  26.8 18.3 %all-to-all-start.1 = ((bf16[128,8,256]{0,2,1:T(8,128)(2,1)}), bf16[128,8,256]{0,2,1:T(8,128)(2,1)S(1)}, u32[]{:S(2)}, u32[]{:S(2)}) async-start(bf16[128,8,256]{0,2,1:T(8,128)(2,1)} %bitcast.5), calls=%async_computation.1 | async-start | bytes 1048576 | tf_op jit(solution)/shard_map/all_to_all | solution.py:134
  33.1 20.1 %copy-start.12 = (bf16[1,128,2048]{2,1,0:T(8,128)(2,1)S(1)}, bf16[1,128,2048]{2,1,0:T(8,128)(2,1)}, u32[]{:S(2)}) copy-start(bf16[1,128,2048]{2,1,0:T(8,128)(2,1)} %param.10) | copy-start | bytes 1572868
  45.1 18.3 %all-to-all-start.3 = ((bf16[128,8,256]{0,2,1:T(8,128)(2,1)}), bf16[128,8,256]{0,2,1:T(8,128)(2,1)S(1)}, u32[]{:S(2)}, u32[]{:S(2)}) async-start(bf16[128,8,256]{0,2,1:T(8,128)(2,1)} %bitcast.20), calls=%async_computation.3 | async-start | bytes 1048576 | tf_op jit(solution)/shard_map/all_to_all | solution.py:135
  63.4 338.6 %all-to-all-start.4 = ((bf16[128,8,256]{0,2,1:T(8,128)(2,1)}), bf16[128,8,256]{0,2,1:T(8,128)(2,1)S(1)}, u32[]{:S(2)}, u32[]{:S(2)}) async-start(bf16[128,8,256]{0,2,1:T(8,128)(2,1)} %bitcast.162), calls=%async_computation.4 | async-start | bytes 1048576 | tf_op jit(solution)/shard_map/all_to_all | solution.py:130
  69.4 1.2 copy-start.7
  69.9 5.1 %copy-start.3 = (f32[4,8,64,128]{3,2,1,0:T(8,128)}, f32[4,8,64,128]{3,2,1,0:T(8,128)S(1)}, u32[]{:S(2)}) copy-start(f32[4,8,64,128]{3,2,1,0:T(8,128)S(1)} %bitcast_multiply_fusion.2) | copy-start | bytes 3145732
  402.0 51.9 %all-to-all-start = ((bf16[128,8,256]{0,2,1:T(8,128)(2,1)}), bf16[128,8,256]{0,2,1:T(8,128)(2,1)}, u32[]{:S(2)}, u32[]{:S(2)}) async-start(bf16[128,8,256]{0,2,1:T(8,128)(2,1)} %bitcast.161), calls=%async_computation | async-start | bytes 1048576 | tf_op jit(solution)/shard_map/all_to_all | solution.py:128
  408.0 3.3 copy-start.9
  408.0 3.3 copy-start.10
  411.3 2.2 copy-start.4
  413.5 2.8 copy-start.1
  414.6 2.8 copy-start.6
  417.4 1.6 copy-start.8
  432.8 11.1 %slice-start = ((f32[4,8,64,64]{3,2,1,0:T(8,128)}), f32[4,1,64,64]{3,2,1,0:T(8,128)S(1)}, s32[]{:S(2)}) async-start(f32[4,8,64,64]{3,2,1,0:T(8,128)} %copy-done.8), calls=%async_computation.7 | async-start | bytes 262144 | tf_op jit(solution)/shard_map/slice | solution.py:94
  453.9 2.8 copy-start.5
  456.7 2.9 copy-start.2
Sparse Core Ops, SparseCore 0:
  17.0 58.2 all-gather.1
where the time goes:
time: 506 us; the launch traced here: 499 us
  other arithmetic  325 us (64%)
  matrix products  45.2 us (9%)
  local copies, waits for them, and re-layouts  38.9 us (8%)
  starting transfers between devices  30 us (6%)
  waiting for transfers between devices  28.7 us (6%)
  blocking collectives  17 us (3%)
  between operations  13.9 us (3%)
    another operation x4, other arithmetic, run_mixer(): jax.scipy.linalg.solve_triangular(lower_matrix, right_sides, lower=True,...  316 us
    dot_general x11, matrix products, product_three(): return jnp.einsum(form, left, right, precision=THREE_PASS)  23.9 us
    all_to_all x1, blocking collectives, per_device(): back = lax.all_to_all(mix, 'sp', split_axis=0, concat_axis=1, tiled=True)  17 us
    unnamed x36, local copies, waits for them, and re-layouts  15.2 us
    dot_general x8, matrix products, product(): return jnp.einsum(form, left, right, precision=HIGHEST)  12.9 us
    all_to_all x1, waiting for transfers between devices, per_device(): lax.all_to_all(decay_pre, 'sp', split_axis=1, concat_axis=0, tiled=True)  10.9 us
    pad x2, local copies, waits for them, and re-layouts, run_mixer(): _, ends = lax.associative_scan(compose, (transfer, added), axis=1)  10.3 us
  transfers between devices with their start and end apart: 6, of which 3 were waited for; matrix products, arithmetic and copies ran while one was open for 80% of the time, Pallas kernels for 0%

commit v1 on v0

v1 whole, which is shorter than its diff:
```python
import functools
import math

import jax
import jax.numpy as jnp
from jax import lax
from jax.experimental import pallas as pl
from jax.experimental.pallas import tpu as pltpu
from jax.sharding import PartitionSpec as P

HEAD = 64
PAIR = 2 * HEAD

F32 = jnp.float32
BF16 = jnp.bfloat16


def mm(left, right):
    return lax.dot_general(left, right, (((1,), (0,)), ((), ())), preferred_element_type=F32)


def mm_nt(left, right):
    return lax.dot_general(left, right, (((1,), (1,)), ((), ())), preferred_element_type=F32)


def mm_tn(left, right):
    return lax.dot_general(left, right, (((0,), (0,)), ((), ())), preferred_element_type=F32)


def split(x):
    high = x.astype(BF16)
    return high, (x - high.astype(F32)).astype(BF16)


def mm3(left, right, form=mm):
    return form(left[0], right[0]) + form(left[0], right[1]) + form(left[1], right[0])


def iota(shape, dim):
    return lax.broadcasted_iota(jnp.int32, shape, dim)


def first_half(shape):
    return iota(shape, len(shape) - 1) < HEAD


def stack_pair(x):
    here = lax.rem(iota(x.shape, 1), PAIR) < HEAD
    zero = jnp.zeros_like(x)
    return jnp.concatenate([jnp.where(here, x, zero), jnp.where(here, zero, x)], axis=0)


def head_ones(scale):
    row = iota((2 * PAIR, PAIR), 0)
    col = iota((2 * PAIR, PAIR), 1)
    same = (lax.rem(row, PAIR) // HEAD) == (col // HEAD)
    return jnp.where(same, F32(scale), F32(0.0)).astype(BF16)


def head_sum(x, ones):
    return mm(jnp.concatenate(split(x), axis=1), ones)


def inverse_levels(strict_parts, size):
    row = iota((size, size), 0)
    col = iota((size, size), 1)
    eye = jnp.where(row == col, F32(1.0), F32(0.0))
    found = None
    block = 1
    while block < size:
        pick = (row // (2 * block) == col // (2 * block)) & (row // block != col // block) & (row > col)
        pieces = [jnp.where(pick, high, jnp.zeros_like(high)) for high, _ in strict_parts]
        if found is None:
            found = [eye.astype(BF16) - p for p in pieces]
        else:
            right = [mm(p, x).astype(BF16) for p, x in zip(pieces, found)]
            found = [x - mm(x, y).astype(BF16) for x, y in zip(found, right)]
        block *= 2
    out = []
    for (high, low), x in zip(strict_parts, found):
        product = mm(jnp.concatenate([high, low], axis=1), jnp.concatenate([x, x], axis=0))
        residual = ((eye - x.astype(F32)) - product).astype(BF16)
        out.append((x, mm(x, residual).astype(BF16)))
    return out


def gates(squashed, rate_low, decay_up, rate_up, base):
    decay_pre = (base + mm(squashed, decay_up)).astype(BF16).astype(F32)
    rate_pre = mm(rate_low, rate_up).astype(BF16).astype(F32)
    log_decay = -math.exp(-0.5) / (1.0 + jnp.exp(-decay_pre))
    rate = 1.0 / (1.0 + jnp.exp(-rate_pre))
    return log_decay, rate


def local_pairs(pairs):
    size = pairs[0][0].shape[0]
    middle = size // 2
    row = iota((size, size), 0)
    col = iota((size, size), 1)
    strict = row > col
    within = row >= col
    upto = jnp.where(within, F32(1.0), F32(0.0)).astype(BF16)
    upto = jnp.concatenate([upto, upto], axis=1)
    ones = head_ones(1.0)
    made = []
    strict_parts = []
    for q, k, v, log_decay, rate in pairs:
        q = q.astype(F32)
        k = k.astype(F32)
        running = mm(upto, jnp.concatenate(split(log_decay), axis=0))
        centre = running[middle : middle + 1]
        final = running[size - 1 :]
        ahead = jnp.exp(running - centre)
        ahead_before = jnp.exp(running - log_decay - centre)
        behind = jnp.exp(centre - running)
        unit = k * lax.rsqrt(1.0 + head_sum(k * k, ones))
        erase = unit * rate
        at_centre = jnp.exp(centre)
        at_end = jnp.exp(final - centre)
        read_mid = q * ahead
        erase_from = unit * ahead_before
        key_to = k * behind
        erase_to = erase * behind
        left = split(jnp.concatenate([stack_pair(erase_from), stack_pair(read_mid)], axis=0))
        right = split(jnp.concatenate([key_to, erase_to], axis=0))
        grid = mm_nt(
            jnp.concatenate(left, axis=1), jnp.concatenate([right[0], right[0]], axis=1)
        ) + mm_nt(left[0], right[1])
        part = lambda i, j, keep: jnp.where(
            keep, grid[i * size : (i + 1) * size, j * size : (j + 1) * size], 0.0
        )
        key_pairs = split(jnp.concatenate([part(0, 0, strict), part(1, 0, strict)], axis=1))
        strict_parts += [split(part(0, 1, strict)), split(part(1, 1, strict))]
        read_keys = split(jnp.concatenate([part(2, 0, within), part(3, 0, within)], axis=1))
        read_erase = split(jnp.concatenate([part(2, 1, within), part(3, 1, within)], axis=1))
        values = stack_pair(v)
        carried = mm(key_pairs[0], values) + mm(key_pairs[1], values)
        kept = mm(read_keys[0], values) + mm(read_keys[1], values)
        sides = jnp.concatenate([erase_from * at_centre, carried], axis=1)
        made.append((
            v, sides, kept, read_erase, read_mid * at_centre,
            key_to * at_end, erase_to * at_end, jnp.exp(final),
        ))
    inverses = inverse_levels(strict_parts, size)
    out = []
    for i, (v, sides, kept, read_erase, read_start, key_end, erase_end, decay_all) in enumerate(made):
        xa, xb = inverses[2 * i], inverses[2 * i + 1]
        inv = tuple(jnp.concatenate([a, b], axis=1) for a, b in zip(xa, xb))
        solved = mm3(inv, split(stack_pair(sides)))
        parts = split(solved)
        taken = mm3(read_erase, tuple(stack_pair(p) for p in parts))
        read_state = read_start - taken[:, :PAIR]
        readout = kept - taken[:, PAIR:]
        key_parts = split(key_end)
        erase_parts = split(erase_end)
        moved = mm3(erase_parts, parts, mm_tn)
        gained = mm_tn(key_parts[0], v) + mm_tn(key_parts[1], v)
        row2 = iota((PAIR, PAIR), 0)
        col2 = iota((PAIR, PAIR), 1)
        transfer = jnp.where(row2 == col2, jnp.broadcast_to(decay_all, (PAIR, PAIR)), 0.0) - moved[:, :PAIR]
        added = gained - moved[:, PAIR:]
        half = first_half((HEAD, PAIR))
        fold = lambda x: jnp.where(half, x[:HEAD], x[HEAD:])
        out.append((fold(transfer), fold(added), read_state, readout))
    return out


def local_kernel(count, q_ref, k_ref, v_ref, low_ref, rate_ref, dup_ref, rup_ref, base_ref,
                 transfer_ref, added_ref, state_ref, readout_ref):
    squashed = jnp.tanh(low_ref[...].astype(F32)).astype(BF16)
    log_decay, rate = gates(squashed, rate_ref[...], dup_ref[...], rup_ref[...], base_ref[...])
    pairs = []
    for i in range(count):
        at = slice(i * PAIR, (i + 1) * PAIR)
        pairs.append((q_ref[:, at], k_ref[:, at], v_ref[:, at], log_decay[:, at], rate[:, at]))
    for i, (transfer, added, state, readout) in enumerate(local_pairs(pairs)):
        at = slice(i * PAIR, (i + 1) * PAIR)
        transfer_ref[:, at] = transfer
        added_ref[:, at] = added
        state_ref[:, at] = state
        readout_ref[:, at] = readout


def local_block(q, k, v, decay_low, rate_low, decay_up, rate_up, base):
    size, width = q.shape
    low = decay_low.shape[1]
    count = math.gcd(width // PAIR, 2)
    lanes = count * PAIR
    cols = lambda rows: pl.BlockSpec((rows, lanes), lambda i: (0, i))
    whole = pl.BlockSpec((size, low), lambda i: (0, 0))
    return pl.pallas_call(
        functools.partial(local_kernel, count),
        grid=(width // lanes,),
        in_specs=[cols(size)] * 3 + [whole] * 2 + [cols(low)] * 2 + [cols(1)],
        out_specs=[cols(HEAD), cols(HEAD), cols(size), cols(size)],
        out_shape=[
            jax.ShapeDtypeStruct((HEAD, width), F32),
            jax.ShapeDtypeStruct((HEAD, width), F32),
            jax.ShapeDtypeStruct((size, width), F32),
            jax.ShapeDtypeStruct((size, width), F32),
        ],
        cost_estimate=pl.CostEstimate(flops=10**10, bytes_accessed=10**7, transcendentals=0),
        name="local_block",
    )(q, k, v, decay_low, rate_low, decay_up, rate_up, base)


def chain_kernel(devices, group, transfer_ref, added_ref, state_ref, readout_ref, gain_ref,
                 mix_ref, start_buf, end_buf, send_sem, recv_sem):
    me = lax.axis_index("sp")
    groups = transfer_ref.shape[1] // group
    has_left = me > 0
    has_right = me < devices - 1
    barrier = pltpu.get_barrier_semaphore()

    @pl.when(has_left)
    def _():
        pl.semaphore_signal(barrier, inc=1, device_id={"sp": me - 1}, device_id_type=pl.DeviceIdType.MESH)

    @pl.when(has_right)
    def _():
        pl.semaphore_signal(barrier, inc=1, device_id={"sp": me + 1}, device_id_type=pl.DeviceIdType.MESH)

    pl.semaphore_wait(barrier, jnp.minimum(me, 1) + jnp.minimum(devices - 1 - me, 1))

    def copy(g):
        return pltpu.make_async_remote_copy(
            src_ref=end_buf.at[g],
            dst_ref=start_buf.at[g],
            send_sem=send_sem.at[g],
            recv_sem=recv_sem.at[g],
            device_id={"sp": lax.rem(me + 1, devices)},
            device_id_type=pl.DeviceIdType.MESH,
        )

    mean_ones = head_ones(1.0 / HEAD)

    @pl.when(jnp.logical_not(has_left))
    def _():
        start_buf[...] = jnp.zeros_like(start_buf)

    for g in range(groups):
        @pl.when(has_left)
        def _():
            copy(g).wait_recv()

        starts = []
        for i in range(group // PAIR):
            at = slice(g * group + i * PAIR, g * group + (i + 1) * PAIR)
            here = slice(i * PAIR, (i + 1) * PAIR)
            start = split(stack_pair(start_buf[g, :, here]))
            end_buf[g, :, here] = mm3(split(transfer_ref[:, at]), start) + added_ref[:, at]
            starts.append(start)

        @pl.when(has_right)
        def _():
            copy(g).start()

        for i, start in enumerate(starts):
            at = slice(g * group + i * PAIR, g * group + (i + 1) * PAIR)
            readout = mm3(split(state_ref[:, at]), start) + readout_ref[:, at]
            centred = readout - head_sum(readout, mean_ones)
            variance = head_sum(centred * centred, mean_ones)
            mix_ref[:, at] = (centred * lax.rsqrt(variance + 1.0) * gain_ref[:, at]).astype(BF16)

    @pl.when(has_right)
    def _():
        for g in range(groups):
            copy(g).wait_send()


def chain(devices, transfer, added, state, readout, gain):
    size, width = state.shape
    group = PAIR * math.gcd(width // PAIR, 2)
    groups = width // group
    vmem = pl.BlockSpec(memory_space=pltpu.VMEM)
    return pl.pallas_call(
        functools.partial(chain_kernel, devices, group),
        in_specs=[vmem] * 5,
        out_specs=vmem,
        out_shape=jax.ShapeDtypeStruct((size, width), BF16),
        scratch_shapes=[
            pltpu.VMEM((groups, HEAD, group), F32),
            pltpu.VMEM((groups, HEAD, group), F32),
            pltpu.SemaphoreType.DMA((groups,)),
            pltpu.SemaphoreType.DMA((groups,)),
        ],
        compiler_params=pltpu.CompilerParams(collective_id=0, has_side_effects=True),
        cost_estimate=pl.CostEstimate(flops=10**10, bytes_accessed=10**7, transcendentals=0),
        name="state_chain",
    )(transfer, added, state, readout, gain)


def per_device(devices, query_rows, key_rows, value_rows, decay_low, rate_low, decay_up, rate_up,
               decay_base, norm_gain, out_weight):
    weight = lax.all_gather(out_weight, "dp", axis=1, tiled=True)
    made = local_block(
        query_rows[0], key_rows[0], value_rows[0], decay_low[0], rate_low[0],
        decay_up, rate_up, decay_base[None],
    )
    mix = chain(devices, *made, norm_gain[None])
    return jnp.dot(mix, weight, preferred_element_type=F32).astype(BF16)[None]


def solution(mesh):
    in_specs = (
        P("dp", "sp", None),
        P("dp", "sp", None),
        P("dp", "sp", None),
        P("dp", "sp", None),
        P("dp", "sp", None),
        P(),
        P(),
        P(),
        P(),
        P(None, "dp"),
    )
    return jax.shard_map(
        functools.partial(per_device, mesh.shape["sp"]),
        mesh=mesh, in_specs=in_specs, out_specs=P("dp", "sp", None), check_vma=False,
    )
```

time: 506 us -> 97.8 us (0.19); the launches traced: 499 us -> 97.6 us
  other arithmetic: 325 us -> 0 us
  Pallas kernels: 0 us -> 77.8 us
  matrix products: 45.2 us -> 5.62 us
  local copies, waits for them, and re-layouts: 38.9 us -> 0 us
  starting transfers between devices: 30 us -> 0.01 us
  waiting for transfers between devices: 28.7 us -> 0.73 us
  blocking collectives: 17 us -> 0 us
    another operation x4 -> x0, other arithmetic: 316 us -> none  [run_mixer(): jax.scipy.linalg.solve_triangular(lower_matrix, right_sides, lower=True,...]
    pallas_call x0 -> x2, Pallas kernels: none -> 77.8 us  [the longest x1 39.2 us: chain(): pl.pallas_call(functools.partial(chain_kernel, devices, group), in_specs=...]
    dot_general x22 -> x1, matrix products: 42.8 us -> 5.62 us  [per_device(): return jnp.dot(mix, weight, preferred_element_type=F32).astype(BF16)[None]]
    all_to_all x5 -> x0, starting transfers between devices: 30 us -> none  [the longest x1 6 us: per_device(): lax.all_to_all(valued, 'sp', split_axis=1, concat_axis=0, tiled=True)]
    all_to_all x5 -> x0, waiting for transfers between devices: 28 us -> none  [the longest x1 10.9 us: per_device(): lax.all_to_all(decay_pre, 'sp', split_axis=1, concat_axis=0, tiled=True)]
    all_to_all x1 -> x0, blocking collectives: 17 us -> none  [per_device(): back = lax.all_to_all(mix, 'sp', split_axis=0, concat_axis=1, tiled=True)]
    unnamed x36 -> x0, local copies, waits for them, and re-layouts: 15.2 us -> none
    pad x2 -> x0, local copies, waits for them, and re-layouts: 10.3 us -> none  [run_mixer(): _, ends = lax.associative_scan(compose, (transfer, added), axis=1)]
  transfers between devices with their start and end apart: 6 -> 1, of which waited for: 3 -> 0; matrix products, arithmetic and copies ran while one was open for 80% -> 0% of each run, Pallas kernels for 0% -> 80%
where the time goes in v1:
time: 97.8 us; the launch traced here: 97.6 us
  Pallas kernels  77.8 us (80%)
  between operations  13.4 us (14%)
  matrix products  5.62 us (6%)
    pallas_call x1, Pallas kernels, chain(): pl.pallas_call(functools.partial(chain_kernel, devices, group), in_specs=...  39.2 us
    pallas_call x1, Pallas kernels, local_block(): pl.pallas_call(functools.partial(local_kernel, count), grid=(width // lan...  38.7 us
    dot_general x1, matrix products, per_device(): return jnp.dot(mix, weight, preferred_element_type=F32).astype(BF16)[None]  5.62 us
  transfers between devices with their start and end apart: 1, of which 0 were waited for; matrix products, arithmetic and copies ran while one was open for 0% of the time, Pallas kernels for 80%

profile of v1, /device:TPU:30, one launch (start us, length us, event | category | flops | bytes accessed | tf_op | source)
XLA Modules:
  0.0 97.6 jit_solution(5288904720411773826)
XLA Ops:
  6.5 0.0 all-gather.2.cloned.1.call-start
  6.5 0.7 all-gather.2.cloned.1.call-update
  7.3 38.7 %local_block.1 = (f32[64,2048]{1,0:T(8,128)}, f32[64,2048]{1,0:T(8,128)}, f32[128,2048]{1,0:T(8,128)}, f32[128,2048]{1,0:T(8,128)}) custom-call(bf16[128,2048]{1,0:T(8,128)(2,1)} %bitcast.11, bf16[128,2048]{1,0:T(8,128)(2,1)} %bitcast.12, bf16[128,2048]{1,0:T(8,128)(2,1)} %bitcast.13, bf16[128,128]{1,0:T(8,128)(2,1)} %bitcast.14, bf16[128,128]{1,0:T(8,128)(2,1)} %bitcast.15, ...), custom_call_target="tpu_custom_call" | custom-call | flops 10000000000 | bytes 10000000 | tf_op jit(solution)/shard_map/local_block/pallas_call | solution.py:191
  45.9 39.2 %state_chain.1 = bf16[128,2048]{1,0:T(8,128)(2,1)} custom-call(f32[64,2048]{1,0:T(8,128)} %get-tuple-element.9.transfer_ref, f32[64,2048]{1,0:T(8,128)} %get-tuple-element.10.added_ref, f32[128,2048]{1,0:T(8,128)} %get-tuple-element.11.state_ref, f32[128,2048]{1,0:T(8,128)} %get-tuple-element.12.readout_ref, f32[1,2048]{1,0:T(1,128)} %bitcast.17), custom_call_target="tpu_custom_call" | custom-call | flops 10000000000 | bytes 10000000 | tf_op jit(solution)/shard_map/state_chain/pallas_call | solution.py:276
  85.1 0.0 all-gather.2.cloned.1.call-done
  85.1 5.6 %fusion = bf16[1,128,2048]{2,1,0:T(8,128)(2,1)} fusion(bf16[128,2048]{1,0:T(8,128)(2,1)} %state_chain.1, bf16[2048,2048]{1,0:T(8,128)(2,1)} %all-gather.2.cloned.1.call-done), kind=kOutput, calls=%fused_computation.1 | convolution fusion | flops 1074003968 | bytes 9437184 | tf_op jit(solution)/shard_map/dot_general | solution.py:301
Async XLA Ops:
  6.5 78.6 %all-gather.2.cloned.1.call-start = ((), (), s32[]{:S(2)}) async-start(), calls=%async_computation | async-start | bytes 10485760 | tf_op jit(solution)/shard_map/all_gather | solution.py:295
Sparse Core Ops, SparseCore 0:
  8.9 58.2 all-gather.1

commit v2 on v1

--- a/solution.py
+++ b/solution.py
@@ -165,71 +165,105 @@
     return out
 
 
-def local_kernel(count, q_ref, k_ref, v_ref, low_ref, rate_ref, dup_ref, rup_ref, base_ref,
-                 transfer_ref, added_ref, state_ref, readout_ref):
-    squashed = jnp.tanh(low_ref[...].astype(F32)).astype(BF16)
-    log_decay, rate = gates(squashed, rate_ref[...], dup_ref[...], rup_ref[...], base_ref[...])
-    pairs = []
-    for i in range(count):
-        at = slice(i * PAIR, (i + 1) * PAIR)
-        pairs.append((q_ref[:, at], k_ref[:, at], v_ref[:, at], log_decay[:, at], rate[:, at]))
-    for i, (transfer, added, state, readout) in enumerate(local_pairs(pairs)):
-        at = slice(i * PAIR, (i + 1) * PAIR)
-        transfer_ref[:, at] = transfer
-        added_ref[:, at] = added
-        state_ref[:, at] = state
-        readout_ref[:, at] = readout
-
-
-def local_block(q, k, v, decay_low, rate_low, decay_up, rate_up, base):
-    size, width = q.shape
-    low = decay_low.shape[1]
-    count = math.gcd(width // PAIR, 2)
-    lanes = count * PAIR
-    cols = lambda rows: pl.BlockSpec((rows, lanes), lambda i: (0, i))
-    whole = pl.BlockSpec((size, low), lambda i: (0, 0))
-    return pl.pallas_call(
-        functools.partial(local_kernel, count),
-        grid=(width // lanes,),
-        in_specs=[cols(size)] * 3 + [whole] * 2 + [cols(low)] * 2 + [cols(1)],
-        out_specs=[cols(HEAD), cols(HEAD), cols(size), cols(size)],
-        out_shape=[
-            jax.ShapeDtypeStruct((HEAD, width), F32),
-            jax.ShapeDtypeStruct((HEAD, width), F32),
-            jax.ShapeDtypeStruct((size, width), F32),
-            jax.ShapeDtypeStruct((size, width), F32),
-        ],
-        cost_estimate=pl.CostEstimate(flops=10**10, bytes_accessed=10**7, transcendentals=0),
-        name="local_block",
-    )(q, k, v, decay_low, rate_low, decay_up, rate_up, base)
-
-
-def chain_kernel(devices, group, transfer_ref, added_ref, state_ref, readout_ref, gain_ref,
-                 mix_ref, start_buf, end_buf, send_sem, recv_sem):
+def fused_kernel(devices, columns, lanes, pieces, q_ref, k_ref, v_ref, low_ref, rate_ref, dup_ref,
+                 rup_ref, base_ref, gain_ref, weight_ref, out_ref, weights, transfer_ref, added_ref,
+                 state_ref, readout_ref, mix_ref, start_buf, end_buf, own_sem, near_sem, far_send,
+                 far_recv, pass_send, pass_recv, send_sem, recv_sem):
     me = lax.axis_index("sp")
-    groups = transfer_ref.shape[1] // group
+    mine = lax.axis_index("dp")
+    partner = mine + 1 - 2 * lax.rem(mine, 2)
+    width = q_ref.shape[1]
+    groups = width // lanes
+    count = lanes // PAIR
+    others = columns // 2 - 1
+    cols = weight_ref.shape[1]
+    piece = weight_ref.shape[0] // pieces
     has_left = me > 0
     has_right = me < devices - 1
     barrier = pltpu.get_barrier_semaphore()
 
+    def greet(where):
+        pl.semaphore_signal(barrier, inc=1, device_id=where, device_id_type=pl.DeviceIdType.MESH)
+
+    def ahead_of(j):
+        return lax.rem(mine + 2 * (j + 1), columns)
+
+    def behind_of(j):
+        return lax.rem(mine + columns - 2 * (j + 1), columns)
+
+    def remote(src, dst, send, recv, where):
+        return pltpu.make_async_remote_copy(
+            src_ref=src, dst_ref=dst, send_sem=send, recv_sem=recv,
+            device_id=where, device_id_type=pl.DeviceIdType.MESH,
+        )
+
+    greet({"dp": partner})
+    for j in range(others):
+        greet({"dp": ahead_of(j)})
+
     @pl.when(has_left)
     def _():
-        pl.semaphore_signal(barrier, inc=1, device_id={"sp": me - 1}, device_id_type=pl.DeviceIdType.MESH)
+        greet({"sp": me - 1})
 
     @pl.when(has_right)
     def _():
-        pl.semaphore_signal(barrier, inc=1, device_id={"sp": me + 1}, device_id_type=pl.DeviceIdType.MESH)
-
-    pl.semaphore_wait(barrier, jnp.minimum(me, 1) + jnp.minimum(devices - 1 - me, 1))
+        greet({"sp": me + 1})
+
+    own = pltpu.make_async_copy(weight_ref, weights.at[mine], own_sem)
+    own.start()
+    pl.semaphore_wait(
+        barrier, 1 + others + jnp.minimum(me, 1) + jnp.minimum(devices - 1 - me, 1)
+    )
+
+    def rows(c):
+        return pl.ds(c * piece, piece)
+
+    def far(j, c):
+        return remote(
+            weight_ref.at[rows(c)], weights.at[mine, rows(c)],
+            far_send.at[j, c], far_recv.at[j, c], {"dp": ahead_of(j)},
+        )
+
+    def passed(j, c):
+        return remote(
+            weights.at[behind_of(j), rows(c)], weights.at[behind_of(j), rows(c)],
+            pass_send.at[j, c], pass_recv.at[j, c], {"dp": partner},
+        )
+
+    near = remote(weight_ref, weights.at[mine], near_sem.at[0], near_sem.at[1], {"dp": partner})
+    for j in range(others):
+        for c in range(pieces):
+            far(j, c).start()
+    near.start()
+
+    def forward(c):
+        for j in range(others):
+            far(j, c).wait_recv()
+            passed(j, c).start()
+
+    def local_step(g, carry):
+        at = pl.ds(pl.multiple_of(g * lanes, lanes), lanes)
+        squashed = jnp.tanh(low_ref[...].astype(F32)).astype(BF16)
+        log_decay, rate = gates(
+            squashed, rate_ref[...], dup_ref[:, at], rup_ref[:, at], base_ref[:, at]
+        )
+        q, k, v = q_ref[:, at], k_ref[:, at], v_ref[:, at]
+        cut = lambda x, i: x[:, i * PAIR : (i + 1) * PAIR]
+        pairs = [tuple(cut(x, i) for x in (q, k, v, log_decay, rate)) for i in range(count)]
+        parts = list(zip(*local_pairs(pairs)))
+        for ref, part in zip((transfer_ref, added_ref, state_ref, readout_ref), parts):
+            ref[:, at] = jnp.concatenate(part, axis=1)
+        return carry
+
+    lax.fori_loop(0, groups, local_step, 0)
+    early = pieces // 2
+    for c in range(early):
+        forward(c)
 
     def copy(g):
-        return pltpu.make_async_remote_copy(
-            src_ref=end_buf.at[g],
-            dst_ref=start_buf.at[g],
-            send_sem=send_sem.at[g],
-            recv_sem=recv_sem.at[g],
-            device_id={"sp": lax.rem(me + 1, devices)},
-            device_id_type=pl.DeviceIdType.MESH,
+        return remote(
+            end_buf.at[g], start_buf.at[g], send_sem.at[g], recv_sem.at[g],
+            {"sp": lax.rem(me + 1, devices)},
         )
 
     mean_ones = head_ones(1.0 / HEAD)
@@ -244,8 +278,8 @@
             copy(g).wait_recv()
 
         starts = []
-        for i in range(group // PAIR):
-            at = slice(g * group + i * PAIR, g * group + (i + 1) * PAIR)
+        for i in range(count):
+            at = slice(g * lanes + i * PAIR, g * lanes + (i + 1) * PAIR)
             here = slice(i * PAIR, (i + 1) * PAIR)
             start = split(stack_pair(start_buf[g, :, here]))
             end_buf[g, :, here] = mm3(split(transfer_ref[:, at]), start) + added_ref[:, at]
@@ -256,49 +290,83 @@
             copy(g).start()
 
         for i, start in enumerate(starts):
-            at = slice(g * group + i * PAIR, g * group + (i + 1) * PAIR)
+            at = slice(g * lanes + i * PAIR, g * lanes + (i + 1) * PAIR)
             readout = mm3(split(state_ref[:, at]), start) + readout_ref[:, at]
             centred = readout - head_sum(readout, mean_ones)
             variance = head_sum(centred * centred, mean_ones)
             mix_ref[:, at] = (centred * lax.rsqrt(variance + 1.0) * gain_ref[:, at]).astype(BF16)
 
+    for c in range(early, pieces):
+        forward(c)
+
+    def project(d):
+        at = pl.ds(pl.multiple_of(d * cols, cols), cols)
+        out_ref[:, at] = mm(mix_ref[...], weights[d]).astype(BF16)
+
+    own.wait()
+    project(mine)
+    near.wait_recv()
+    project(partner)
+    for j in range(others):
+        project(behind_of(j))
+    for j in range(others):
+        for c in range(pieces):
+            passed(j, c).wait_recv()
+        project(lax.rem(partner + columns - 2 * (j + 1), columns))
+
+    near.wait_send()
+    for j in range(others):
+        for c in range(pieces):
+            far(j, c).wait_send()
+            passed(j, c).wait_send()
+
     @pl.when(has_right)
     def _():
         for g in range(groups):
             copy(g).wait_send()
 
 
-def chain(devices, transfer, added, state, readout, gain):
-    size, width = state.shape
-    group = PAIR * math.gcd(width // PAIR, 2)
-    groups = width // group
+def per_device(devices, columns, query_rows, key_rows, value_rows, decay_low, rate_low, decay_up,
+               rate_up, decay_base, norm_gain, out_weight):
+    q = query_rows[0]
+    size, width = q.shape
+    depth, cols = out_weight.shape
+    lanes = PAIR * math.gcd(width // PAIR, 2)
+    groups = width // lanes
+    pieces = 4
+    others = columns // 2 - 1
     vmem = pl.BlockSpec(memory_space=pltpu.VMEM)
-    return pl.pallas_call(
-        functools.partial(chain_kernel, devices, group),
-        in_specs=[vmem] * 5,
+    dma = lambda *dims: pltpu.SemaphoreType.DMA(dims)
+    out = pl.pallas_call(
+        functools.partial(fused_kernel, devices, columns, lanes, pieces),
+        in_specs=[vmem] * 9 + [pl.BlockSpec(memory_space=pl.ANY)],
         out_specs=vmem,
-        out_shape=jax.ShapeDtypeStruct((size, width), BF16),
+        out_shape=jax.ShapeDtypeStruct((size, columns * cols), BF16),
         scratch_shapes=[
-            pltpu.VMEM((groups, HEAD, group), F32),
-            pltpu.VMEM((groups, HEAD, group), F32),
-            pltpu.SemaphoreType.DMA((groups,)),
-            pltpu.SemaphoreType.DMA((groups,)),
+            pltpu.VMEM((columns, depth, cols), BF16),
+            pltpu.VMEM((HEAD, width), F32),
+            pltpu.VMEM((HEAD, width), F32),
+            pltpu.VMEM((size, width), F32),
+            pltpu.VMEM((size, width), F32),
+            pltpu.VMEM((size, width), BF16),
+            pltpu.VMEM((groups, HEAD, lanes), F32),
+            pltpu.VMEM((groups, HEAD, lanes), F32),
+            pltpu.SemaphoreType.DMA,
+            dma(2),
+            dma(others, pieces),
+            dma(others, pieces),
+            dma(others, pieces),
+            dma(others, pieces),
+            dma(groups),
+            dma(groups),
         ],
         compiler_params=pltpu.CompilerParams(collective_id=0, has_side_effects=True),
-        cost_estimate=pl.CostEstimate(flops=10**10, bytes_accessed=10**7, transcendentals=0),
-        name="state_chain",
-    )(transfer, added, state, readout, gain)
-
-
-def per_device(devices, query_rows, key_rows, value_rows, decay_low, rate_low, decay_up, rate_up,
-               decay_base, norm_gain, out_weight):
-    weight = lax.all_gather(out_weight, "dp", axis=1, tiled=True)
-    made = local_block(
-        query_rows[0], key_rows[0], value_rows[0], decay_low[0], rate_low[0],
-        decay_up, rate_up, decay_base[None],
+        name="fused_mixer",
+    )(
+        q, key_rows[0], value_rows[0], decay_low[0], rate_low[0], decay_up, rate_up,
+        decay_base[None], norm_gain[None], out_weight,
     )
-    mix = chain(devices, *made, norm_gain[None])
-    return jnp.dot(mix, weight, preferred_element_type=F32).astype(BF16)[None]
+    return out[None]
 
 
 def solution(mesh):
@@ -315,6 +383,6 @@
         P(None, "dp"),
     )
     return jax.shard_map(
-        functools.partial(per_device, mesh.shape["sp"]),
+        functools.partial(per_device, mesh.shape["sp"], mesh.shape["dp"]),
         mesh=mesh, in_specs=in_specs, out_specs=P("dp", "sp", None), check_vma=False,
     )

time: 97.8 us -> 81.4 us (0.83); the launches traced: 97.6 us -> 80.2 us
  between operations: 13.4 us -> 0.01 us
  matrix products: 5.62 us -> 0 us
  local copies, waits for them, and re-layouts: 0 us -> 1.88 us
    dot_general x1 -> x0, matrix products: 5.62 us -> none  [per_device(): return jnp.dot(mix, weight, preferred_element_type=F32).astype(BF16)[None]]
    unnamed x0 -> x1, local copies, waits for them, and re-layouts: none -> 1.88 us
    pallas_call x2 -> x1, Pallas kernels: 77.8 us -> 78.3 us  [per_device(): pl.pallas_call(functools.partial(fused_kernel, devices, columns, lanes, p...]
  transfers between devices with their start and end apart: 1 -> 0, of which waited for: 0 -> 0; matrix products, arithmetic and copies ran while one was open for 0% -> 0% of each run, Pallas kernels for 80% -> 0%
where the time goes in v2:
time: 81.4 us; the launch traced here: 80.2 us
  Pallas kernels  78.3 us (96%)
  local copies, waits for them, and re-layouts  1.88 us (2%)
    pallas_call x1, Pallas kernels, per_device(): pl.pallas_call(functools.partial(fused_kernel, devices, columns, lanes, p...  78.3 us
    unnamed x1, local copies, waits for them, and re-layouts  1.88 us

profile of v2, /device:TPU:30, one launch (start us, length us, event | category | flops | bytes accessed | tf_op | source)
XLA Modules:
  0.0 80.2 jit_solution(13900731549656404474)
XLA Ops:
  0.0 78.3 %fused_mixer.1 = bf16[128,2048]{1,0:T(8,128)(2,1)} custom-call(bf16[128,2048]{1,0:T(8,128)(2,1)} %bitcast.9, bf16[128,2048]{1,0:T(8,128)(2,1)} %bitcast.10, bf16[128,2048]{1,0:T(8,128)(2,1)} %bitcast.11, bf16[128,128]{1,0:T(8,128)(2,1)} %bitcast.12, bf16[128,128]{1,0:T(8,128)(2,1)} %bitcast.13, bf16[128,2048]{1,0:T(8,128)(2,1)} %dup_ref.1, ...), custom_call_target="tpu_custom_call" | custom-call | tf_op jit(solution)/shard_map/fused_mixer/pallas_call | solution.py:340
  78.3 1.9 %copy.12 = bf16[1,128,2048]{2,1,0:T(8,128)(2,1)} copy(bf16[1,128,2048]{2,1,0:T(8,128)(2,1)} %bitcast.8) | data formatting | bytes 1048576

commit v3 on v2

--- a/solution.py
+++ b/solution.py
@@ -92,68 +92,53 @@
     return log_decay, rate
 
 
-def local_pairs(pairs):
+def state_pairs(pairs):
     size = pairs[0][0].shape[0]
     middle = size // 2
     row = iota((size, size), 0)
     col = iota((size, size), 1)
     strict = row > col
-    within = row >= col
-    upto = jnp.where(within, F32(1.0), F32(0.0)).astype(BF16)
+    upto = jnp.where(row >= col, F32(1.0), F32(0.0)).astype(BF16)
     upto = jnp.concatenate([upto, upto], axis=1)
     ones = head_ones(1.0)
     made = []
     strict_parts = []
-    for q, k, v, log_decay, rate in pairs:
-        q = q.astype(F32)
+    for k, v, log_decay, rate in pairs:
         k = k.astype(F32)
         running = mm(upto, jnp.concatenate(split(log_decay), axis=0))
         centre = running[middle : middle + 1]
         final = running[size - 1 :]
-        ahead = jnp.exp(running - centre)
         ahead_before = jnp.exp(running - log_decay - centre)
         behind = jnp.exp(centre - running)
         unit = k * lax.rsqrt(1.0 + head_sum(k * k, ones))
-        erase = unit * rate
-        at_centre = jnp.exp(centre)
         at_end = jnp.exp(final - centre)
-        read_mid = q * ahead
         erase_from = unit * ahead_before
         key_to = k * behind
-        erase_to = erase * behind
-        left = split(jnp.concatenate([stack_pair(erase_from), stack_pair(read_mid)], axis=0))
-        right = split(jnp.concatenate([key_to, erase_to], axis=0))
-        grid = mm_nt(
-            jnp.concatenate(left, axis=1), jnp.concatenate([right[0], right[0]], axis=1)
-        ) + mm_nt(left[0], right[1])
-        part = lambda i, j, keep: jnp.where(
-            keep, grid[i * size : (i + 1) * size, j * size : (j + 1) * size], 0.0
-        )
-        key_pairs = split(jnp.concatenate([part(0, 0, strict), part(1, 0, strict)], axis=1))
-        strict_parts += [split(part(0, 1, strict)), split(part(1, 1, strict))]
-        read_keys = split(jnp.concatenate([part(2, 0, within), part(3, 0, within)], axis=1))
-        read_erase = split(jnp.concatenate([part(2, 1, within), part(3, 1, within)], axis=1))
+        erase_to = unit * rate * behind
+        left = split(stack_pair(erase_from))
+        key_parts, erase_parts = split(key_to), split(erase_to)
+        right = [jnp.concatenate(both, axis=0) for both in zip(key_parts, erase_parts)]
+        grid = pair_grid(left, right)
+        part = lambda i, j: jnp.where(
+            strict, grid[i * size : (i + 1) * size, j * size : (j + 1) * size], 0.0
+        )
+        key_pairs = split(jnp.concatenate([part(0, 0), part(1, 0)], axis=1))
+        strict_parts += [split(part(0, 1)), split(part(1, 1))]
         values = stack_pair(v)
         carried = mm(key_pairs[0], values) + mm(key_pairs[1], values)
-        kept = mm(read_keys[0], values) + mm(read_keys[1], values)
-        sides = jnp.concatenate([erase_from * at_centre, carried], axis=1)
+        sides = jnp.concatenate([erase_from * jnp.exp(centre), carried], axis=1)
         made.append((
-            v, sides, kept, read_erase, read_mid * at_centre,
-            key_to * at_end, erase_to * at_end, jnp.exp(final),
+            v, sides, key_to * at_end, erase_to * at_end, jnp.exp(final),
+            running, key_parts + erase_parts,
         ))
     inverses = inverse_levels(strict_parts, size)
     out = []
-    for i, (v, sides, kept, read_erase, read_start, key_end, erase_end, decay_all) in enumerate(made):
+    for i, (v, sides, key_end, erase_end, decay_all, running, kept) in enumerate(made):
         xa, xb = inverses[2 * i], inverses[2 * i + 1]
         inv = tuple(jnp.concatenate([a, b], axis=1) for a, b in zip(xa, xb))
-        solved = mm3(inv, split(stack_pair(sides)))
-        parts = split(solved)
-        taken = mm3(read_erase, tuple(stack_pair(p) for p in parts))
-        read_state = read_start - taken[:, :PAIR]
-        readout = kept - taken[:, PAIR:]
+        solved = split(mm3(inv, split(stack_pair(sides))))
         key_parts = split(key_end)
-        erase_parts = split(erase_end)
-        moved = mm3(erase_parts, parts, mm_tn)
+        moved = mm3(split(erase_end), solved, mm_tn)
         gained = mm_tn(key_parts[0], v) + mm_tn(key_parts[1], v)
         row2 = iota((PAIR, PAIR), 0)
         col2 = iota((PAIR, PAIR), 1)
@@ -161,13 +146,44 @@
         added = gained - moved[:, PAIR:]
         half = first_half((HEAD, PAIR))
         fold = lambda x: jnp.where(half, x[:HEAD], x[HEAD:])
-        out.append((fold(transfer), fold(added), read_state, readout))
+        halves = tuple(x[:, j : j + PAIR] for j in (0, PAIR) for x in solved)
+        out.append((fold(transfer), fold(added), running) + kept + halves)
     return out
+
+
+def pair_grid(left, right):
+    return mm_nt(
+        jnp.concatenate(left, axis=1), jnp.concatenate([right[0], right[0]], axis=1)
+    ) + mm_nt(left[0], right[1])
+
+
+def read_pair(q, v, running, kept, start, mean_ones):
+    size = q.shape[0]
+    within = iota((size, size), 0) >= iota((size, size), 1)
+    centre = running[size // 2 : size // 2 + 1]
+    read_mid = q.astype(F32) * jnp.exp(running - centre)
+    left = split(stack_pair(read_mid))
+    right = [jnp.concatenate([kept[i], kept[i + 2]], axis=0) for i in (0, 1)]
+    solved = [jnp.concatenate([kept[i + 4], kept[i + 6]], axis=1) for i in (0, 1)]
+    grid = pair_grid(left, right)
+    part = lambda i, j: jnp.where(
+        within, grid[i * size : (i + 1) * size, j * size : (j + 1) * size], 0.0
+    )
+    read_keys = split(jnp.concatenate([part(0, 0), part(1, 0)], axis=1))
+    read_erase = split(jnp.concatenate([part(0, 1), part(1, 1)], axis=1))
+    values = stack_pair(v)
+    here = mm(read_keys[0], values) + mm(read_keys[1], values)
+    taken = mm3(read_erase, [stack_pair(x) for x in solved])
+    read_state = read_mid * jnp.exp(centre) - taken[:, :PAIR]
+    readout = mm3(split(read_state), split(stack_pair(start))) + here - taken[:, PAIR:]
+    centred = readout - head_sum(readout, mean_ones)
+    variance = head_sum(centred * centred, mean_ones)
+    return centred * lax.rsqrt(variance + 1.0)
 
 
 def fused_kernel(devices, columns, lanes, pieces, q_ref, k_ref, v_ref, low_ref, rate_ref, dup_ref,
                  rup_ref, base_ref, gain_ref, weight_ref, out_ref, weights, transfer_ref, added_ref,
-                 state_ref, readout_ref, mix_ref, start_buf, end_buf, own_sem, near_sem, far_send,
+                 running_ref, kept_ref, mix_ref, start_buf, end_buf, own_sem, near_sem, far_send,
                  far_recv, pass_send, pass_recv, send_sem, recv_sem):
     me = lax.axis_index("sp")
     mine = lax.axis_index("dp")
@@ -241,24 +257,24 @@
             far(j, c).wait_recv()
             passed(j, c).start()
 
-    def local_step(g, carry):
-        at = pl.ds(pl.multiple_of(g * lanes, lanes), lanes)
+    def lanes_of(g):
+        return pl.ds(pl.multiple_of(g * lanes, lanes), lanes)
+
+    def cut(x, i):
+        return x[:, i * PAIR : (i + 1) * PAIR]
+
+    def make(g):
+        at = lanes_of(g)
         squashed = jnp.tanh(low_ref[...].astype(F32)).astype(BF16)
         log_decay, rate = gates(
             squashed, rate_ref[...], dup_ref[:, at], rup_ref[:, at], base_ref[:, at]
         )
-        q, k, v = q_ref[:, at], k_ref[:, at], v_ref[:, at]
-        cut = lambda x, i: x[:, i * PAIR : (i + 1) * PAIR]
-        pairs = [tuple(cut(x, i) for x in (q, k, v, log_decay, rate)) for i in range(count)]
-        parts = list(zip(*local_pairs(pairs)))
-        for ref, part in zip((transfer_ref, added_ref, state_ref, readout_ref), parts):
-            ref[:, at] = jnp.concatenate(part, axis=1)
-        return carry
-
-    lax.fori_loop(0, groups, local_step, 0)
-    early = pieces // 2
-    for c in range(early):
-        forward(c)
+        k, v = k_ref[:, at], v_ref[:, at]
+        pairs = [tuple(cut(x, i) for x in (k, v, log_decay, rate)) for i in range(count)]
+        parts = [jnp.concatenate(part, axis=1) for part in zip(*state_pairs(pairs))]
+        transfer_ref[:, at], added_ref[:, at], running_ref[:, at] = parts[:3]
+        for i, part in enumerate(parts[3:]):
+            kept_ref[i, :, at] = part
 
     def copy(g):
         return remote(
@@ -266,36 +282,70 @@
             {"sp": lax.rem(me + 1, devices)},
         )
 
+    def advance(g):
+        @pl.when(has_left)
+        def _():
+            copy(g).wait_recv()
+
+        at = lanes_of(g)
+        transfer, added, start = transfer_ref[:, at], added_ref[:, at], start_buf[g]
+        ends = [
+            mm3(split(cut(transfer, i)), split(stack_pair(cut(start, i)))) for i in range(count)
+        ]
+        end_buf[g] = jnp.concatenate(ends, axis=1) + added
+
+        @pl.when(has_right)
+        def _():
+            copy(g).start()
+
     mean_ones = head_ones(1.0 / HEAD)
+
+    def read(g):
+        at = lanes_of(g)
+        q, v, running, gain, start = (
+            q_ref[:, at], v_ref[:, at], running_ref[:, at], gain_ref[:, at], start_buf[g]
+        )
+        kept = [kept_ref[j, :, at] for j in range(kept_ref.shape[0])]
+        normed = [
+            read_pair(
+                cut(q, i), cut(v, i), cut(running, i), [cut(x, i) for x in kept],
+                cut(start, i), mean_ones,
+            )
+            for i in range(count)
+        ]
+        mix_ref[:, at] = (jnp.concatenate(normed, axis=1) * gain).astype(BF16)
 
     @pl.when(jnp.logical_not(has_left))
     def _():
         start_buf[...] = jnp.zeros_like(start_buf)
 
-    for g in range(groups):
-        @pl.when(has_left)
-        def _():
-            copy(g).wait_recv()
-
-        starts = []
-        for i in range(count):
-            at = slice(g * lanes + i * PAIR, g * lanes + (i + 1) * PAIR)
-            here = slice(i * PAIR, (i + 1) * PAIR)
-            start = split(stack_pair(start_buf[g, :, here]))
-            end_buf[g, :, here] = mm3(split(transfer_ref[:, at]), start) + added_ref[:, at]
-            starts.append(start)
-
-        @pl.when(has_right)
-        def _():
-            copy(g).start()
-
-        for i, start in enumerate(starts):
-            at = slice(g * lanes + i * PAIR, g * lanes + (i + 1) * PAIR)
-            readout = mm3(split(state_ref[:, at]), start) + readout_ref[:, at]
-            centred = readout - head_sum(readout, mean_ones)
-            variance = head_sum(centred * centred, mean_ones)
-            mix_ref[:, at] = (centred * lax.rsqrt(variance + 1.0) * gain_ref[:, at]).astype(BF16)
-
+    slots = max(groups, devices) + groups
+    early = min(pieces, (slots - 1) // 4)
+
+    def slot(s, carry):
+        @pl.when(s < groups)
+        def _():
+            make(s)
+
+        @pl.when((s >= me) & (s < me + groups))
+        def _():
+            advance(s - me)
+
+        first = jnp.maximum(groups, me + 1)
+
+        @pl.when((s >= first) & (s < first + groups))
+        def _():
+            read(s - first)
+
+        c = s // 4 - 1
+
+        @pl.when((lax.rem(s, 4) == 0) & (c >= 0) & (c < early))
+        def _():
+            forward(c)
+
+        return carry
+
+    lax.fori_loop(0, slots, slot, 0)
     for c in range(early, pieces):
         forward(c)
 
@@ -347,7 +397,7 @@
             pltpu.VMEM((HEAD, width), F32),
             pltpu.VMEM((HEAD, width), F32),
             pltpu.VMEM((size, width), F32),
-            pltpu.VMEM((size, width), F32),
+            pltpu.VMEM((8, size, width), BF16),
             pltpu.VMEM((size, width), BF16),
             pltpu.VMEM((groups, HEAD, lanes), F32),
             pltpu.VMEM((groups, HEAD, lanes), F32),

time: 81.4 us -> 69.3 us (0.85)
  Pallas kernels: 78.3 us -> 66.3 us
    pallas_call x1, Pallas kernels: 78.3 us -> 66.3 us  [per_device(): pl.pallas_call(functools.partial(fused_kernel, devices, columns, lanes, p...]
where the time goes in v3:
time: 69.3 us; the launch traced here: 68.2 us
  Pallas kernels  66.3 us (96%)
  local copies, waits for them, and re-layouts  1.88 us (3%)
    pallas_call x1, Pallas kernels, per_device(): pl.pallas_call(functools.partial(fused_kernel, devices, columns, lanes, p...  66.3 us
    unnamed x1, local copies, waits for them, and re-layouts  1.88 us

profile of v3, /device:TPU:30, one launch (start us, length us, event | category | flops | bytes accessed | tf_op | source)
XLA Modules:
  0.0 68.2 jit_solution(4223556825301929474)
XLA Ops:
  0.0 66.3 %fused_mixer.1 = bf16[128,2048]{1,0:T(8,128)(2,1)} custom-call(bf16[128,2048]{1,0:T(8,128)(2,1)} %bitcast.9, bf16[128,2048]{1,0:T(8,128)(2,1)} %bitcast.10, bf16[128,2048]{1,0:T(8,128)(2,1)} %bitcast.11, bf16[128,128]{1,0:T(8,128)(2,1)} %bitcast.12, bf16[128,128]{1,0:T(8,128)(2,1)} %bitcast.13, bf16[128,2048]{1,0:T(8,128)(2,1)} %dup_ref.1, ...), custom_call_target="tpu_custom_call" | custom-call | tf_op jit(solution)/shard_map/fused_mixer/pallas_call | solution.py:390
  66.3 1.9 %copy.12 = bf16[1,128,2048]{2,1,0:T(8,128)(2,1)} copy(bf16[1,128,2048]{2,1,0:T(8,128)(2,1)} %bitcast.8) | data formatting | bytes 1048576
